TPU v7x, 32 devices: a whole 2x2x4 slice. The times are simulated.
32 devices in a mesh: ep: 4 (over z), tp: 8 (over y, x, core).
Axes of the slice: x: 2, y: 2, z: 4, core: 2. Of those that a mesh axis runs over, the one named last changes fastest.
Arguments:
- tokens: bfloat16 [1024, 2048], P('ep'), may hold values from -6 to 6
- norm_gain: float32 [2048], replicated, may hold values from 0.1 to 1.9
- expert_ids: int32 [1024, 2], P('ep'), may hold values from 0 to 3, all different within a row; in each aligned block of 256 rows (0 to 255, 256 to 511, ...) at most 192 rows name the same one
- routing_weight: float32 [1024, 2], P('ep'), may hold values from 0.1 to 1
- expert_gate: bfloat16 [4, 2048, 5632], P('ep', None, 'tp'), may hold values from -0.125 to 0.125
- expert_up: bfloat16 [4, 2048, 5632], P('ep', None, 'tp'), may hold values from -0.125 to 0.125
- expert_down: bfloat16 [4, 5632, 2048], P('ep', 'tp'), may hold values from -0.078125 to 0.078125
- dense_gate_w: bfloat16 [2048, 1024], P(None, 'tp'), may hold values from -0.125 to 0.125
- dense_up_w: bfloat16 [2048, 1024], P(None, 'tp'), may hold values from -0.125 to 0.125
- dense_down_w: bfloat16 [1024, 2048], P('tp'), may hold values from -0.1875 to 0.1875
- dense_gate: float32 [2048], P('tp'), may hold values from -3 to 3
Outputs:
- layer_out: bfloat16 [1024, 2048], P('ep', 'tp')
Inputs may be any that keep to these rules, and one draw needn't show every extreme that they name: `expert_ids`: within the 256 rows of one device along ep, each row names two different experts and no expert is named by more than 192 rows; some expert is named by exactly 192 rows.
All inputs are finite; a program needn't handle non-finite values.
Results may differ from a plain program's by a relative error of at most 0.017.
Values may be sent and summed in bfloat16 or wider, within the bound.
A program may use at most 64 MiB of HBM per device.

v0:
```python
import jax
import jax.numpy as jnp
from jax import lax
from jax.sharding import PartitionSpec as P

EPSILON = 1e-06


def positions(block_ids, experts, capacity):
    flat_ids = block_ids.reshape(-1)
    one_hot = (flat_ids[:, None] == jnp.arange(experts, dtype=jnp.int32)[None, :]).astype(jnp.int32)
    earlier = jnp.cumsum(one_hot, axis=0) - one_hot
    return flat_ids * capacity + jnp.sum(earlier * one_hot, axis=1)


def transposed_term(hidden, down_w):
    return lax.dot_general(
        down_w, hidden, (((0,), (1,)), ((), ())), preferred_element_type=jnp.float32
    )


def local(
    tokens,
    norm_gain,
    expert_ids,
    routing_weight,
    expert_gate,
    expert_up,
    expert_down,
    dense_gate_w,
    dense_up_w,
    dense_down_w,
    dense_gate,
):
    experts = lax.axis_size("ep")
    group_tokens, model_width = tokens.shape
    capacity = 3 * group_tokens // experts
    slots_all = experts * capacity
    part_rows = model_width // lax.axis_size("tp")
    values = tokens.astype(jnp.float32)
    factor = lax.rsqrt(jnp.mean(values * values, axis=-1, keepdims=True) + EPSILON)
    normed = (values * factor * norm_gain[None, :]).astype(jnp.bfloat16)
    places = positions(expert_ids, experts, capacity)
    token_no = jnp.arange(2 * group_tokens, dtype=jnp.int32) // 2 + 1
    sources = jnp.zeros((slots_all,), jnp.int32).at[places].set(token_no)
    padded = jnp.concatenate([jnp.zeros((1, model_width), jnp.bfloat16), normed], axis=0)
    gate_w = expert_gate[0]
    up_w = expert_up[0]
    down_w = expert_down[0]
    first_col = lax.axis_index("tp") * part_rows
    column_part = lax.dynamic_slice_in_dim(padded, first_col, part_rows, 1)
    outgoing = column_part[sources].reshape(experts, capacity, part_rows)
    landed = lax.all_to_all(outgoing, "ep", split_axis=0, concat_axis=0, tiled=True)
    portion = lax.all_gather(landed, "tp", axis=2, tiled=True)
    columns = portion.reshape(slots_all, portion.shape[2])
    gate_act = jnp.dot(columns, gate_w, preferred_element_type=jnp.float32)
    up_act = jnp.dot(columns, up_w, preferred_element_type=jnp.float32)
    hidden = (jax.nn.silu(gate_act) * up_act).astype(jnp.bfloat16)
    dense_gate_act = jnp.dot(normed, dense_gate_w, preferred_element_type=jnp.float32)
    dense_up_act = jnp.dot(normed, dense_up_w, preferred_element_type=jnp.float32)
    dense_hidden = (jax.nn.silu(dense_gate_act) * dense_up_act).astype(jnp.bfloat16)
    dense_out = lax.psum_scatter(
        transposed_term(dense_hidden, dense_down_w).astype(jnp.bfloat16),
        "tp",
        scatter_dimension=0,
        tiled=True,
    ).astype(jnp.float32)
    expert_out = lax.psum_scatter(
        transposed_term(hidden, down_w).astype(jnp.bfloat16), "tp", scatter_dimension=0, tiled=True
    )
    expert_half = expert_out.reshape(part_rows, experts, capacity)
    returned = lax.all_to_all(expert_half, "ep", split_axis=1, concat_axis=1, tiled=True).reshape(
        part_rows, slots_all
    )
    picked = (
        jnp.take(returned, places, axis=1).astype(jnp.float32).reshape(part_rows, group_tokens, 2)
    )
    routed = jnp.sum(picked * routing_weight[None, :, :], axis=2)
    gate_factor = jax.nn.sigmoid(dense_gate)[:, None]
    return (routed + gate_factor * dense_out).T.astype(jnp.bfloat16)


def solution(mesh):
    return jax.shard_map(
        local,
        mesh=mesh,
        in_specs=(
            P("ep", None),
            P(),
            P("ep", None),
            P("ep", None),
            P("ep", None, "tp"),
            P("ep", None, "tp"),
            P("ep", "tp", None),
            P(None, "tp"),
            P(None, "tp"),
            P("tp", None),
            P("tp"),
        ),
        out_specs=P("ep", "tp"),
        check_vma=False,
    )
```

profile of v0, /device:TPU:0, one launch (start us, length us, event | category | flops | bytes accessed | tf_op | source)
XLA Modules:
  0.0 181.6 jit_solution(7366420034769287310)
XLA Ops:
  6.5 0.0 copy-start
  6.5 0.0 all-gather.2.cloned.1.call-start
  6.5 0.8 broadcast_multiply_fusion
  7.4 0.8 copy.18
  8.2 0.1 eq.26
  8.4 0.1 reshape.85
  8.5 1.5 fusion.7
  10.0 0.1 copy.22
  10.2 0.1 mul.83
  10.4 1.2 reduce-window.6
  11.6 0.2 slice_reduce_fusion
  11.8 0.2 reduce-window.9
  12.0 0.1 add_bitcast_fusion
  12.1 2.4 %scatter_custom_fusion = s32[768]{0:T(1024)S(1)} fusion(s32[512]{0:T(512)S(1)} %bitcast.60, s32[512]{0:T(512)S(1)} %fusion.26, s32[]{:T(128)} %constant.29.clone.1), kind=kCustom, calls=%fused_computation.53 | custom fusion | bytes 3076 | tf_op jit(solution)/shard_map/scatter | solution.py:45
  14.6 1.5 fusion.9
  16.1 0.0 copy-start.1
  16.1 1.0 copy-done.1
  17.2 0.1 pad_dynamic-slice_fusion
  17.3 2.7 %gather_fusion = bf16[768,256]{1,0:T(8,128)(2,1)S(1)} fusion(bf16[257,256]{1,0:T(8,128)(2,1)S(1)} %pad_dynamic-slice_fusion, s32[1024]{0:T(1024)S(1)} %pad_clamp_fusion.1), kind=kCustom, calls=%fused_computation | custom fusion | bytes 789504 | tf_op jit(solution)/shard_map/gather | solution.py:52
  20.0 17.9 %all_to_all.10 = bf16[4,192,256]{2,1,0:T(8,128)(2,1)} all-to-all(bf16[4,192,256]{2,1,0:T(8,128)(2,1)S(1)} %bitcast.56), channel_id=1, replica_groups=mesh['ep'=4,'tp'=8] {'ep'}, dimensions={0} | all-to-all | bytes 786432 | tf_op jit(solution)/shard_map/all_to_all | solution.py:53
  37.9 0.0 all-gather.2.cloned.1.call-update
  37.9 0.0 reduce-scatter.3.cloned.1.call-start
  38.0 31.9 %all-gather.2.cloned.1.call-done = bf16[4,192,2048]{2,1,0:T(8,128)(2,1)} async-done(((bf16[4,192,256]{2,1,0:T(8,128)(2,1)}), bf16[4,192,2048]{2,1,0:T(8,128)(2,1)}) %all-gather.2.cloned.1.call-update) | async-done | bytes 3145744 | tf_op jit(solution)/shard_map/all_gather | solution.py:54
  69.9 6.6 %fusion.4 = f32[768,704]{0,1:T(8,128)} fusion(bf16[768,2048]{1,0:T(8,128)(2,1)} %bitcast.63, bf16[1,2048,704]{1,2,0:T(8,128)(2,1)} %param.15), kind=kOutput, calls=%fused_computation.8 | convolution fusion | flops 2214592512 | bytes 8192000 | tf_op jit(solution)/shard_map/dot_general | solution.py:56
  76.5 0.0 copy-done
  76.5 11.6 %fusion = bf16[2048,768]{0,1:T(8,128)(2,1)} fusion(bf16[1,704,2048]{2,1,0:T(8,128)(2,1)S(1)} %copy-done, f32[768,704]{0,1:T(8,128)} %fusion.4, bf16[768,2048]{1,0:T(8,128)(2,1)} %bitcast.64, bf16[1,2048,704]{1,2,0:T(8,128)(2,1)} %param.16), kind=kOutput, calls=%fused_computation.4 | convolution fusion | flops 4434001920 | bytes 14221312 | tf_op jit(solution)/shard_map/dot_general | solution.py:17
  88.1 0.0 reduce-scatter.3.cloned.1.call-update
  88.1 0.2 reduce-scatter.5.cloned.1.call-start
  88.3 1.8 fusion.34
  90.1 0.0 copy-done.2
  90.1 0.0 copy-start.3
  90.1 0.0 copy-start.4
  90.1 3.1 %fusion.6 = bf16[2048,256]{0,1:T(8,128)(2,1)} fusion(bf16[128,2048]{1,0:T(8,128)(2,1)S(1)} %copy-done.2, bf16[256,2048]{1,0:T(8,128)(2,1)} %copy-done.1, bf16[2048,128]{1,0:T(8,128)(2,1)} %param.19, f32[256,128]{1,0:T(8,128)S(1)} %fusion.34), kind=kOutput, calls=%fused_computation.13 | convolution fusion | flops 269156352 | bytes 3276800 | tf_op jit(solution)/shard_map/dot_general | solution.py:17
  93.3 0.0 reduce-scatter.5.cloned.1.call-update
  93.3 41.0 %reduce-scatter.3.cloned.1.call-done = bf16[256,768]{0,1:T(8,128)(2,1)} async-done(((bf16[2048,768]{0,1:T(8,128)(2,1)}), bf16[256,768]{0,1:T(8,128)(2,1)}) %reduce-scatter.3.cloned.1.call-update) | async-done | bytes 393232 | tf_op jit(solution)/shard_map/reduce_scatter | solution.py:68
  134.3 4.6 %all-to-all-start.1 = ((bf16[256,4,192]{0,2,1:T(8,128)(2,1)}), bf16[256,4,192]{0,2,1:T(8,128)(2,1)S(1)}, u32[]{:S(2)}, u32[]{:S(2)}) async-start(bf16[256,4,192]{0,2,1:T(8,128)(2,1)} %bitcast.58), calls=%async_computation.2 | async-start | bytes 786432 | tf_op jit(solution)/shard_map/all_to_all | solution.py:72
  138.9 0.1 reduce_sum.32
  139.0 0.1 copy.20
  139.1 0.0 copy-done.3
  139.1 0.8 copy.21
  139.9 0.1 copy.23
  140.1 0.7 add_divide_fusion
  140.7 9.6 %all-to-all-done.1 = bf16[256,4,192]{0,2,1:T(8,128)(2,1)S(1)} async-done(((bf16[256,4,192]{0,2,1:T(8,128)(2,1)}), bf16[256,4,192]{0,2,1:T(8,128)(2,1)S(1)}, u32[]{:S(2)}, u32[]{:S(2)}) %all-to-all-start.1) | async-done | bytes 393248 | tf_op jit(solution)/shard_map/all_to_all | solution.py:72
  150.4 2.6 %gather_fusion.1 = bf16[512,256]{1,0:T(8,128)(2,1)} fusion(bf16[256,768]{0,1:T(8,128)(2,1)S(1)} %bitcast.55, s32[1024]{0:T(1024)S(1)} %pad_clamp_fusion), kind=kCustom, calls=%fused_computation.1 | custom fusion | bytes 526336 | tf_op jit(solution)/shard_map/jit(_take)/gather | solution.py:76
  153.0 1.1 gather.11
  154.0 2.2 %multiply_reduce_fusion = f32[256,256]{0,1:T(8,128)S(1)} fusion(bf16[256,256,2]{0,2,1:T(2,128)(2,1)S(1)} %gather.11, pred[256,2]{1,0:T(8,128)(4,1)} %copy.21, f32[256,2]{1,0:T(8,128)S(1)} %copy.23), kind=kLoop, calls=%fused_computation.21 | loop fusion | flops 458752 | bytes 526848 | tf_op jit(solution)/shard_map/reduce_sum | solution.py:78
  156.2 17.2 %reduce-scatter.5.cloned.1.call-done = bf16[256,256]{0,1:T(8,128)(2,1)} async-done(((bf16[2048,256]{0,1:T(8,128)(2,1)}), bf16[256,256]{0,1:T(8,128)(2,1)}) %reduce-scatter.5.cloned.1.call-update) | async-done | bytes 131088 | tf_op jit(solution)/shard_map/reduce_scatter | solution.py:62
  173.5 1.6 fusion.15
  (11 shorter events, 0.1 us)
Async XLA Ops:
  6.5 69.9 %copy-start = (bf16[1,704,2048]{2,1,0:T(8,128)(2,1)S(1)}, bf16[1,704,2048]{2,1,0:T(8,128)(2,1)}, u32[]{:S(2)}) copy-start(bf16[1,704,2048]{2,1,0:T(8,128)(2,1)} %param.17) | copy-start | bytes 8650756
  6.5 63.4 %all-gather.2.cloned.1.call-start = ((), (), s32[]{:S(2)}) async-start(), calls=%async_computation.4 | async-start | bytes 3538944 | tf_op jit(solution)/shard_map/all_gather | solution.py:54
  16.1 1.1 copy-start.1
  37.9 96.4 %reduce-scatter.3.cloned.1.call-start = ((), (), s32[]{:S(2)}) async-start(), calls=%async_computation.5 | async-start | bytes 3538944 | tf_op jit(solution)/shard_map/reduce_scatter | solution.py:68
  88.1 2.0 %copy-start.2 = (bf16[128,2048]{1,0:T(8,128)(2,1)S(1)}, bf16[128,2048]{1,0:T(8,128)(2,1)}, u32[]{:S(2)}) copy-start(bf16[128,2048]{1,0:T(8,128)(2,1)} %param.20) | copy-start | bytes 1572868
  88.1 85.4 %reduce-scatter.5.cloned.1.call-start = ((), (), s32[]{:S(2)}) async-start(), calls=%async_computation.6 | async-start | bytes 1179648 | tf_op jit(solution)/shard_map/reduce_scatter | solution.py:62
  90.1 49.0 %copy-start.3 = (s32[256,2]{0,1:T(2,128)S(1)}, s32[256,2]{0,1:T(2,128)}, u32[]{:S(2)}) copy-start(s32[256,2]{0,1:T(2,128)} %param.13) | copy-start | bytes 6148
  90.1 49.8 %copy-start.4 = (f32[256,2]{0,1:T(2,128)S(1)}, f32[256,2]{0,1:T(2,128)}, u32[]{:S(2)}) copy-start(f32[256,2]{0,1:T(2,128)} %param.14) | copy-start | bytes 6148
  134.3 16.1 %all-to-all-start.1 = ((bf16[256,4,192]{0,2,1:T(8,128)(2,1)}), bf16[256,4,192]{0,2,1:T(8,128)(2,1)S(1)}, u32[]{:S(2)}, u32[]{:S(2)}) async-start(bf16[256,4,192]{0,2,1:T(8,128)(2,1)} %bitcast.58), calls=%async_computation.2 | async-start | bytes 786432 | tf_op jit(solution)/shard_map/all_to_all | solution.py:72
Sparse Core Ops, SparseCore 0:
  38.0 31.8 all-gather.1
  88.2 46.0 reduce-scatter.2
  137.5 35.9 reduce-scatter.4
where the time goes:
time: 182 us
  waiting for transfers between devices  99.9 us (55%)
  matrix products  23.1 us (13%)
  blocking collectives  17.9 us (10%)
  between operations  13.3 us (7%)
  local copies, waits for them, and re-layouts  12.7 us (7%)
  other arithmetic  9.93 us (5%)
  starting transfers between devices  4.86 us (3%)
    reduce_scatter x1, waiting for transfers between devices, local(): lax.psum_scatter(transposed_term(hidden, down_w).astype(jnp.bfloat16), 't...  41 us
    all_gather x1, waiting for transfers between devices, local(): portion = lax.all_gather(landed, 'tp', axis=2, tiled=True)  31.9 us
    all_to_all x1, blocking collectives, local(): lax.all_to_all(outgoing, 'ep', split_axis=0, concat_axis=0, tiled=True)  17.9 us
    reduce_scatter x1, waiting for transfers between devices, local(): lax.psum_scatter(transposed_term(dense_hidden, dense_down_w).astype(jnp.b...  17.2 us
    dot_general x2, matrix products, transposed_term(): lax.dot_general(down_w, hidden, (((0,), (1,)), ((), ())), preferred_eleme...  14.7 us
    all_to_all x1, waiting for transfers between devices, local(): lax.all_to_all(expert_half, 'ep', split_axis=1, concat_axis=1, tiled=True)  9.65 us
    dot_general x1, matrix products, local(): gate_act = jnp.dot(columns, gate_w, preferred_element_type=jnp.float32)  6.57 us
    all_to_all x1, starting transfers between devices, local(): lax.all_to_all(expert_half, 'ep', split_axis=1, concat_axis=1, tiled=True)  4.59 us
  transfers between devices with their start and end apart: 4, of which 4 were waited for; matrix products, arithmetic and copies ran while one was open for 7% of the time, Pallas kernels for 0%

commit v1 on v0

--- a/solution.py
+++ b/solution.py
@@ -1,6 +1,9 @@
+import functools
 import jax
 import jax.numpy as jnp
 from jax import lax
+from jax.experimental import pallas as pl
+from jax.experimental.pallas import tpu as pltpu
 from jax.sharding import PartitionSpec as P
 
 EPSILON = 1e-06
@@ -19,7 +22,7 @@
     )
 
 
-def local(
+def plain_local(
     tokens,
     norm_gain,
     expert_ids,
@@ -80,6 +83,470 @@
     return (routed + gate_factor * dense_out).T.astype(jnp.bfloat16)
 
 
+BF = jnp.bfloat16
+F32 = jnp.float32
+
+
+def silu_mul(gate_act, up_act):
+    return (gate_act / (1.0 + jnp.exp(-gate_act)) * up_act).astype(BF)
+
+
+def fused_kernel(
+    experts,
+    tok_ref,
+    gain_ref,
+    ids_ref,
+    rw_ref,
+    gw_hbm,
+    uw_hbm,
+    dw_hbm,
+    dg_hbm,
+    du_hbm,
+    dd_hbm,
+    dgate_ref,
+    out_ref,
+    gw,
+    uw,
+    dw,
+    dgu,
+    dd,
+    normed,
+    slot_row,
+    slot_col,
+    gates,
+    zsend,
+    xloc,
+    xbuf,
+    hid,
+    dhid,
+    part_l,
+    part_c,
+    r0_l,
+    r0_c,
+    r1a_l,
+    r1b_l,
+    r1a_c,
+    r1b_c,
+    r2a_l,
+    r2b_l,
+    r2a_c,
+    r2b_c,
+    fin,
+    ret,
+    total,
+    wsem,
+    gsem,
+    zsem,
+    agsem,
+    rssem,
+    retsem,
+):
+    me = lax.axis_index("ep")
+    tp = lax.axis_index("tp")
+    core, xx, yy = tp % 2, (tp // 2) % 2, tp // 4
+    group, width = tok_ref.shape
+    cols = out_ref.shape[1]
+    cap = zsend.shape[1]
+    ffp = gw.shape[1]
+    dsp = dd.shape[0]
+    rounds = experts - 1
+    mesh_id = pl.DeviceIdType.MESH
+
+    def peer(flip):
+        bits = (core + flip % 2) % 2, (xx + flip // 2 % 2) % 2, (yy + flip // 4) % 2
+        return bits[2] * 4 + bits[1] * 2 + bits[0]
+
+    def ring(d):
+        return lax.rem(me + d, experts)
+
+    barrier = pltpu.get_barrier_semaphore()
+    for flip in range(1, 8):
+        pl.semaphore_signal(barrier, 1, device_id=(me, peer(flip)), device_id_type=mesh_id)
+    for d in range(1, experts):
+        pl.semaphore_signal(barrier, 1, device_id=(ring(d), tp), device_id_type=mesh_id)
+
+    loads = [
+        pltpu.make_async_copy(gw_hbm.at[0], gw, wsem.at[0]),
+        pltpu.make_async_copy(uw_hbm.at[0], uw, wsem.at[1]),
+        pltpu.make_async_copy(dg_hbm, dgu.at[:, pl.ds(0, dsp)], wsem.at[2]),
+        pltpu.make_async_copy(du_hbm, dgu.at[:, pl.ds(dsp, dsp)], wsem.at[3]),
+        pltpu.make_async_copy(dw_hbm.at[0], dw, wsem.at[4]),
+        pltpu.make_async_copy(dd_hbm, dd, wsem.at[5]),
+    ]
+    for load in loads:
+        load.start()
+
+    gain = gain_ref[...]
+    step = 32
+
+    def norm_rows(i, carry):
+        rows = pl.ds(pl.multiple_of(i * step, step), step)
+        values = tok_ref[rows, :].astype(F32)
+        factor = lax.rsqrt(jnp.sum(values * values, axis=1, keepdims=True) * (1.0 / width) + EPSILON)
+        normed[rows, :] = (values * factor * gain).astype(BF)
+        return carry
+
+    lax.fori_loop(0, group // step, norm_rows, 0)
+
+    ids = ids_ref[...]
+    id0, id1 = ids[:, 0:1], ids[:, 1:2]
+    lane = lax.broadcasted_iota(jnp.int32, (group, 128), 1)
+    named = (id0 == lane) | (id1 == lane)
+    marks = jnp.where(named, 1.0, 0.0)
+    earlier = jnp.where(
+        lax.broadcasted_iota(jnp.int32, (group, group), 1)
+        < lax.broadcasted_iota(jnp.int32, (group, group), 0),
+        1.0,
+        0.0,
+    ).astype(BF)
+    count = jnp.dot(earlier, marks.astype(BF), preferred_element_type=F32)
+    slots = jnp.where(named, count, -1.0)
+    slot_col[...] = slots
+    slot_row[...] = slots.T
+
+    def pick(e):
+        row = slot_row[pl.ds(e, 1), :].astype(jnp.int32)
+        where = lax.broadcasted_iota(jnp.int32, (cap, group), 0)
+        return jnp.where(row == where, 1.0, 0.0).astype(BF)
+
+    def combine(e):
+        slot = jnp.sum(jnp.where(lane == e, slot_col[...], 0.0), axis=1, keepdims=True).astype(jnp.int32)
+        rw = rw_ref[...]
+        weight = jnp.where(id0 == e, rw[:, 0:1], 0.0) + jnp.where(id1 == e, rw[:, 1:2], 0.0)
+        where = lax.broadcasted_iota(jnp.int32, (group, cap), 1)
+        full = jnp.where(slot == where, weight, 0.0)
+        high = full.astype(BF)
+        return high, (full - high.astype(F32)).astype(BF)
+
+    def mix(pair, rows):
+        return jnp.dot(pair[0], rows, preferred_element_type=F32) + jnp.dot(
+            pair[1], rows, preferred_element_type=F32
+        )
+
+    pl.semaphore_wait(barrier, 7 + rounds)
+
+    pending = []
+
+    def send(src, dst, sems, index, target):
+        copy = pltpu.make_async_remote_copy(
+            src_ref=src,
+            dst_ref=dst,
+            send_sem=sems.at[(0,) + index],
+            recv_sem=sems.at[(1,) + index],
+            device_id=target,
+            device_id_type=mesh_id,
+        )
+        copy.start()
+        pending.append(copy)
+        return copy
+
+    def at_tp(flip):
+        return (me, peer(flip))
+
+    def span(slice_no):
+        return pl.ds(pl.multiple_of(slice_no * cols, cols), cols)
+
+    zcopies, order = {}, list(range(1, experts))
+    if rounds == 3:
+        order = [1, 3, 2]
+    for d in order:
+        rows = jnp.dot(pick(ring(d)), normed[:, span(tp)], preferred_element_type=F32)
+        zsend[d - 1] = rows.astype(BF)
+        zcopies[d] = send(zsend.at[d - 1], xbuf.at[d - 1, :, span(tp)], zsem, (d - 1,), (ring(d), tp))
+    gcopies = [send(dgate_ref, gates.at[tp], gsem, (f - 1,), at_tp(f)) for f in range(1, 8)]
+    gates[tp] = dgate_ref[...]
+    here = pick(me)
+
+    def local_rows(k, carry):
+        at = pl.ds(pl.multiple_of(k * cols, cols), cols)
+        xloc[:, at] = jnp.dot(here, normed[:, at], preferred_element_type=F32).astype(BF)
+        return carry
+
+    lax.fori_loop(0, width // cols, local_rows, 0)
+
+    half = cap // 2
+    top, bottom = pl.ds(0, half), pl.ds(half, half)
+    everything = pl.ds(0, cap)
+    ag = {}
+
+    def move(d, name, number, rows, slice_flip, flip):
+        ref = xbuf.at[d - 1, rows, span(peer(slice_flip))]
+        ag[d, name] = send(ref, ref, agsem, (d - 1, number), at_tp(flip))
+
+    def ag1(d):
+        zcopies[d].wait_recv()
+        move(d, "x", 0, everything, 0, 2)
+        move(d, "y", 1, everything, 0, 4)
+        move(d, "c", 2, everything, 0, 1)
+
+    def ag2(d):
+        ag[d, "x"].wait_recv()
+        move(d, "xy", 3, top, 2, 4)
+        move(d, "xc", 4, everything, 2, 1)
+        ag[d, "y"].wait_recv()
+        move(d, "yx", 5, bottom, 4, 2)
+        move(d, "yc", 6, everything, 4, 1)
+
+    def ag3(d):
+        ag[d, "xy"].wait_recv()
+        move(d, "xyc", 7, top, 6, 1)
+        ag[d, "yx"].wait_recv()
+        move(d, "yxc", 8, bottom, 6, 1)
+
+    def ag_done(d):
+        for name in ("c", "xc", "yc", "xyc", "yxc"):
+            ag[d, name].wait_recv()
+
+    tiles = [(n, min(256, ffp - n)) for n in range(0, ffp, 256)]
+
+    def hidden(rows_ref):
+        for n, size in tiles:
+            gate_act = jnp.dot(rows_ref[...], gw[:, n : n + size], preferred_element_type=F32)
+            up_act = jnp.dot(rows_ref[...], uw[:, n : n + size], preferred_element_type=F32)
+            hid[:, n : n + size] = silu_mul(gate_act, up_act)
+
+    def rs_refs(b):
+        if b == 0:
+            return part_l, r0_l, r1a_l, r1b_l, r2a_l, r2b_l
+        return tuple(r.at[b - 1] for r in (part_c, r0_c, r1a_c, r1b_c, r2a_c, r2b_c))
+
+    rs = {}
+
+    def rs0(b):
+        part, r0 = rs_refs(b)[:2]
+        rs[b, 0] = send(part.at[1 - core], r0, rssem, (b, 0), at_tp(1))
+
+    def add(dst, index, other):
+        dst[index] = (dst[index].astype(F32) + other.astype(F32)).astype(BF)
+
+    def rs1(b):
+        part, r0, r1a, r1b = rs_refs(b)[:4]
+        h = part.shape[3] // 2
+        rs[b, 0].wait_recv()
+        for q in range(4):
+            add(part, (core, q // 2, q % 2), r0[q // 2, q % 2])
+        rs[b, 1] = send(part.at[core, :, 1 - xx, pl.ds(0, h)], r1a, rssem, (b, 1), at_tp(2))
+        rs[b, 2] = send(part.at[core, 1 - yy, :, pl.ds(h, h)], r1b, rssem, (b, 2), at_tp(4))
+
+    def rs2(b):
+        part, r0, r1a, r1b, r2a, r2b = rs_refs(b)
+        h = part.shape[3] // 2
+        rs[b, 1].wait_recv()
+        add(part, (core, 1 - yy, xx, pl.ds(0, h)), r1a[1 - yy])
+        rs[b, 3] = send(part.at[core, 1 - yy, xx, pl.ds(0, h)], r2a, rssem, (b, 3), at_tp(4))
+        rs[b, 2].wait_recv()
+        add(part, (core, yy, 1 - xx, pl.ds(h, h)), r1b[1 - xx])
+        rs[b, 4] = send(part.at[core, yy, 1 - xx, pl.ds(h, h)], r2b, rssem, (b, 4), at_tp(2))
+
+    def rs3(b):
+        part, r0, r1a, r1b, r2a, r2b = rs_refs(b)
+        h = part.shape[3] // 2
+        rs[b, 3].wait_recv()
+        upper = part[core, yy, xx, pl.ds(0, h)].astype(F32) + r1a[yy].astype(F32) + r2a[...].astype(F32)
+        if b == 0:
+            total[pl.ds(0, h), :] = upper
+        else:
+            fin[b - 1, pl.ds(0, h), :] = upper.astype(BF)
+        rs[b, 4].wait_recv()
+        lower = part[core, yy, xx, pl.ds(h, h)].astype(F32) + r1b[xx].astype(F32) + r2b[...].astype(F32)
+        if b == 0:
+            total[pl.ds(h, h), :] = lower
+        else:
+            fin[b - 1, pl.ds(h, h), :] = lower.astype(BF)
+            back = lax.rem(me + experts - b, experts)
+            rs[b, 5] = send(fin.at[b - 1], ret.at[b - 1], retsem, (b - 1,), (back, tp))
+
+    def partials(b):
+        part = rs_refs(b)[0]
+
+        def one(which):
+            def body(q, carry):
+                at = span(2 * q + which)
+                value = jnp.dot(hid[...], dw[:, at], preferred_element_type=F32)
+                part[which, q // 2, q % 2] = value.astype(BF)
+                return carry
+
+            lax.fori_loop(0, 4, body, 0)
+
+        one(1 - core)
+        rs0(b)
+        one(core)
+
+    def dense_partials():
+        pair = combine(me)
+
+        def one(which):
+            def body(q, carry):
+                k = 2 * q + which
+                at = span(k)
+                value = jnp.dot(hid[...], dw[:, at], preferred_element_type=F32).astype(BF)
+                side = jnp.dot(dhid[...], dd[:, at], preferred_element_type=F32)
+                part_l[which, q // 2, q % 2] = (
+                    mix(pair, value) + jax.nn.sigmoid(gates[k]) * side
+                ).astype(BF)
+                return carry
+
+            lax.fori_loop(0, 4, body, 0)
+
+        one(1 - core)
+        rs0(0)
+        one(core)
+
+    def returned(b):
+        rs[b, 5].wait_recv()
+        total[...] += mix(combine(ring(b)), ret[b - 1])
+
+    first, second, third = order
+    ag1(first)
+    loads[0].wait()
+    loads[1].wait()
+    hidden(xloc)
+    ag1(second)
+    loads[2].wait()
+    loads[3].wait()
+    acts = jnp.dot(normed[...], dgu[...], preferred_element_type=F32)
+    dhid[...] = silu_mul(acts[:, :dsp], acts[:, dsp:])
+    ag1(third)
+    ag2(first)
+    loads[4].wait()
+    loads[5].wait()
+    for copy in gcopies:
+        copy.wait_recv()
+    dense_partials()
+    ag2(second)
+    ag3(first)
+    rs1(0)
+    ag_done(first)
+    hidden(xbuf.at[first - 1])
+    ag2(third)
+    ag3(second)
+    partials(first)
+    rs2(0)
+    ag3(third)
+    rs1(first)
+    ag_done(second)
+    hidden(xbuf.at[second - 1])
+    rs3(0)
+    partials(second)
+    rs2(first)
+    rs1(second)
+    ag_done(third)
+    hidden(xbuf.at[third - 1])
+    rs3(first)
+    partials(third)
+    rs2(second)
+    rs1(third)
+    rs3(second)
+    returned(first)
+    rs2(third)
+    returned(second)
+    rs3(third)
+    returned(third)
+    out_ref[...] = total[...].astype(BF)
+    for copy in pending:
+        copy.wait_send()
+
+
+def fused_local(
+    tokens,
+    norm_gain,
+    expert_ids,
+    routing_weight,
+    expert_gate,
+    expert_up,
+    expert_down,
+    dense_gate_w,
+    dense_up_w,
+    dense_down_w,
+    dense_gate,
+):
+    experts = lax.axis_size("ep")
+    parts = lax.axis_size("tp")
+    group, width = tokens.shape
+    cap = 3 * group // experts
+    cols = width // parts
+    ffp = expert_gate.shape[2]
+    dsp = dense_gate_w.shape[1]
+    rounds = experts - 1
+    vmem, hbm = pl.BlockSpec(memory_space=pltpu.VMEM), pl.BlockSpec(memory_space=pl.ANY)
+    dma = pltpu.SemaphoreType.DMA
+    half, ghalf = cap // 2, group // 2
+    return pl.pallas_call(
+        functools.partial(fused_kernel, experts),
+        out_shape=jax.ShapeDtypeStruct((group, cols), BF),
+        in_specs=[vmem] * 4 + [hbm] * 6 + [vmem],
+        out_specs=vmem,
+        scratch_shapes=[
+            pltpu.VMEM((width, ffp), BF),
+            pltpu.VMEM((width, ffp), BF),
+            pltpu.VMEM((ffp, width), BF),
+            pltpu.VMEM((width, 2 * dsp), BF),
+            pltpu.VMEM((dsp, width), BF),
+            pltpu.VMEM((group, width), BF),
+            pltpu.VMEM((128, group), F32),
+            pltpu.VMEM((group, 128), F32),
+            pltpu.VMEM((parts, 1, cols), F32),
+            pltpu.VMEM((rounds, cap, cols), BF),
+            pltpu.VMEM((cap, width), BF),
+            pltpu.VMEM((rounds, cap, width), BF),
+            pltpu.VMEM((cap, ffp), BF),
+            pltpu.VMEM((group, dsp), BF),
+            pltpu.VMEM((2, 2, 2, group, cols), BF),
+            pltpu.VMEM((rounds, 2, 2, 2, cap, cols), BF),
+            pltpu.VMEM((2, 2, group, cols), BF),
+            pltpu.VMEM((rounds, 2, 2, cap, cols), BF),
+            pltpu.VMEM((2, ghalf, cols), BF),
+            pltpu.VMEM((2, ghalf, cols), BF),
+            pltpu.VMEM((rounds, 2, half, cols), BF),
+            pltpu.VMEM((rounds, 2, half, cols), BF),
+            pltpu.VMEM((ghalf, cols), BF),
+            pltpu.VMEM((ghalf, cols), BF),
+            pltpu.VMEM((rounds, half, cols), BF),
+            pltpu.VMEM((rounds, half, cols), BF),
+            pltpu.VMEM((rounds, cap, cols), BF),
+            pltpu.VMEM((rounds, cap, cols), BF),
+            pltpu.VMEM((group, cols), F32),
+            dma((6,)),
+            dma((2, parts - 1)),
+            dma((2, rounds)),
+            dma((2, rounds, 9)),
+            dma((2, experts, 5)),
+            dma((2, rounds)),
+        ],
+        compiler_params=pltpu.CompilerParams(
+            collective_id=0, has_side_effects=True, vmem_limit_bytes=56 * 1024 * 1024
+        ),
+        name="routed_layer",
+    )(
+        tokens,
+        norm_gain[None, :],
+        expert_ids,
+        routing_weight,
+        expert_gate,
+        expert_up,
+        expert_down,
+        dense_gate_w,
+        dense_up_w,
+        dense_down_w,
+        dense_gate[None, :],
+    )
+
+
+def local(*args):
+    experts, parts = lax.axis_size("ep"), lax.axis_size("tp")
+    group, width = args[0].shape
+    fits = (
+        experts == 4
+        and parts == 8
+        and width % (128 * parts) == 0
+        and group % 128 == 0
+        and (3 * group // experts) % 32 == 0
+        and args[7].shape[1] % 128 == 0
+        and args[4].shape[2] % 16 == 0
+    )
+    return (fused_local if fits else plain_local)(*args)
+
+
 def solution(mesh):
     return jax.shard_map(
         local,

time: 182 us -> 70 us (0.38)
  waiting for transfers between devices: 99.9 us -> 0 us
  Pallas kernels: 0 us -> 57.6 us
  matrix products: 23.1 us -> 0 us
  blocking collectives: 17.9 us -> 0 us
  between operations: 13.3 us -> 0.01 us
  other arithmetic: 9.93 us -> 0 us
  starting transfers between devices: 4.86 us -> 0 us
    reduce_scatter x2 -> x0, waiting for transfers between devices: 58.2 us -> none  [the longest x1 41 us: local(): lax.psum_scatter(transposed_term(hidden, down_w).astype(jnp.bfloat16), 't...]
    pallas_call x0 -> x1, Pallas kernels: none -> 57.6 us  [fused_local(): pl.pallas_call(functools.partial(fused_kernel, experts), out_shape=jax.Sh...]
    all_gather x1 -> x0, waiting for transfers between devices: 31.9 us -> none  [local(): portion = lax.all_gather(landed, 'tp', axis=2, tiled=True)]
    dot_general x4 -> x0, matrix products: 23.1 us -> none  [the longest x2 14.7 us: transposed_term(): lax.dot_general(down_w, hidden, (((0,), (1,)), ((), ())), preferred_eleme...]
    all_to_all x1 -> x0, blocking collectives: 17.9 us -> none  [local(): lax.all_to_all(outgoing, 'ep', split_axis=0, concat_axis=0, tiled=True)]
    unnamed x12 -> x7, local copies, waits for them, and re-layouts: 2.04 us -> 12.1 us
    all_to_all x1 -> x0, waiting for transfers between devices: 9.65 us -> none  [local(): lax.all_to_all(expert_half, 'ep', split_axis=1, concat_axis=1, tiled=True)]
    gather x3 -> x0, local copies, waits for them, and re-layouts: 6.27 us -> none  [the longest x2 3.62 us: local(): jnp.take(returned, places, axis=1).astype(jnp.float32)]
  transfers between devices with their start and end apart: 4 -> 0, of which waited for: 4 -> 0; matrix products, arithmetic and copies ran while one was open for 7% -> 0% of each run, Pallas kernels for 0% -> 0%
where the time goes in v1:
time: 70 us; the launch traced here: 69.7 us
  Pallas kernels  57.6 us (82%)
  local copies, waits for them, and re-layouts  12.1 us (17%)
    pallas_call x1, Pallas kernels, fused_local(): pl.pallas_call(functools.partial(fused_kernel, experts), out_shape=jax.Sh...  57.6 us
    unnamed x7, local copies, waits for them, and re-layouts  12.1 us

profile of v1, /device:TPU:0, one launch (start us, length us, event | category | flops | bytes accessed | tf_op | source)
XLA Modules:
  0.0 69.7 jit_solution(11714520295633074079)
XLA Ops:
  0.0 1.5 %copy.12.ids_ref = s32[256,2]{1,0:T(8,128)} copy(s32[256,2]{0,1:T(2,128)} %param.13) | data formatting | bytes 4096 | tf_op args[2]
  1.5 1.5 %copy.13.rw_ref = f32[256,2]{1,0:T(8,128)} copy(f32[256,2]{0,1:T(2,128)} %param.14) | data formatting | bytes 4096 | tf_op args[3]
  2.9 0.0 copy-start
  3.0 4.7 %copy.14.gw_hbm = bf16[1,2048,704]{2,1,0:T(8,128)(2,1)} copy(bf16[1,2048,704]{1,2,0:T(8,128)(2,1)} %param.15) | data formatting | bytes 5767168 | tf_op args[4]
  7.7 0.0 copy-done
  7.7 2.8 %copy.15.uw_hbm = bf16[1,2048,704]{2,1,0:T(8,128)(2,1)} copy(bf16[1,2048,704]{1,2,0:T(8,128)(2,1)S(1)} %copy-done) | data formatting | bytes 5767168 | tf_op args[5]
  10.5 57.6 %routed_layer.1 = bf16[256,256]{1,0:T(8,128)(2,1)} custom-call(bf16[256,2048]{1,0:T(8,128)(2,1)} %tok_ref.1, f32[1,2048]{1,0:T(1,128)} %bitcast.2, s32[256,2]{1,0:T(8,128)} %copy.12.ids_ref, f32[256,2]{1,0:T(8,128)} %copy.13.rw_ref, bf16[1,2048,704]{2,1,0:T(8,128)(2,1)} %copy.14.gw_hbm, bf16[1,2048,704]{2,1,0:T(8,128)(2,1)} %copy.15.uw_hbm, ...), custom_call_target="tpu_custom_call" | custom-call | tf_op jit(solution)/shard_map/routed_layer/pallas_call | solution.py:474
  68.2 1.6 %copy.17 = bf16[256,256]{1,0:T(8,128)(2,1)} copy(bf16[256,256]{1,0:T(8,128)(2,1)} %routed_layer.1) | data formatting | bytes 262144
Async XLA Ops:
  2.9 4.8 %copy-start = (bf16[1,2048,704]{1,2,0:T(8,128)(2,1)S(1)}, bf16[1,2048,704]{1,2,0:T(8,128)(2,1)}, u32[]{:S(2)}) copy-start(bf16[1,2048,704]{1,2,0:T(8,128)(2,1)} %param.16) | copy-start | bytes 8650756

commit v2 on v1

--- a/solution.py
+++ b/solution.py
@@ -91,6 +91,10 @@
     return (gate_act / (1.0 + jnp.exp(-gate_act)) * up_act).astype(BF)
 
 
+def dot_t(rows, weights):
+    return lax.dot_general(rows, weights, (((1,), (1,)), ((), ())), preferred_element_type=F32)
+
+
 def fused_kernel(
     experts,
     tok_ref,
@@ -113,6 +117,7 @@
     normed,
     slot_row,
     slot_col,
+    weight_col,
     gates,
     zsend,
     xloc,
@@ -147,7 +152,7 @@
     group, width = tok_ref.shape
     cols = out_ref.shape[1]
     cap = zsend.shape[1]
-    ffp = gw.shape[1]
+    ffp = gw.shape[0]
     dsp = dd.shape[0]
     rounds = experts - 1
     mesh_id = pl.DeviceIdType.MESH
@@ -188,21 +193,23 @@
 
     lax.fori_loop(0, group // step, norm_rows, 0)
 
-    ids = ids_ref[...]
-    id0, id1 = ids[:, 0:1], ids[:, 1:2]
-    lane = lax.broadcasted_iota(jnp.int32, (group, 128), 1)
-    named = (id0 == lane) | (id1 == lane)
-    marks = jnp.where(named, 1.0, 0.0)
+    id0, id1 = ids_ref[0:1, :], ids_ref[1:2, :]
+    number = lax.broadcasted_iota(jnp.int32, (128, group), 0)
+    named = (id0 == number) | (id1 == number)
     earlier = jnp.where(
-        lax.broadcasted_iota(jnp.int32, (group, group), 1)
-        < lax.broadcasted_iota(jnp.int32, (group, group), 0),
+        lax.broadcasted_iota(jnp.int32, (group, group), 0)
+        < lax.broadcasted_iota(jnp.int32, (group, group), 1),
         1.0,
         0.0,
     ).astype(BF)
-    count = jnp.dot(earlier, marks.astype(BF), preferred_element_type=F32)
+    marks = jnp.where(named, 1.0, 0.0).astype(BF)
+    count = jnp.dot(marks, earlier, preferred_element_type=F32)
     slots = jnp.where(named, count, -1.0)
-    slot_col[...] = slots
-    slot_row[...] = slots.T
+    weights = jnp.where(id0 == number, rw_ref[0:1, :], 0.0) + jnp.where(id1 == number, rw_ref[1:2, :], 0.0)
+    slot_row[...] = slots
+    slot_col[...] = slots.T
+    weight_col[...] = weights.T
+    lane = lax.broadcasted_iota(jnp.int32, (group, 128), 1)
 
     def pick(e):
         row = slot_row[pl.ds(e, 1), :].astype(jnp.int32)
@@ -211,8 +218,7 @@
 
     def combine(e):
         slot = jnp.sum(jnp.where(lane == e, slot_col[...], 0.0), axis=1, keepdims=True).astype(jnp.int32)
-        rw = rw_ref[...]
-        weight = jnp.where(id0 == e, rw[:, 0:1], 0.0) + jnp.where(id1 == e, rw[:, 1:2], 0.0)
+        weight = jnp.sum(jnp.where(lane == e, weight_col[...], 0.0), axis=1, keepdims=True)
         where = lax.broadcasted_iota(jnp.int32, (group, cap), 1)
         full = jnp.where(slot == where, weight, 0.0)
         high = full.astype(BF)
@@ -301,8 +307,8 @@
 
     def hidden(rows_ref):
         for n, size in tiles:
-            gate_act = jnp.dot(rows_ref[...], gw[:, n : n + size], preferred_element_type=F32)
-            up_act = jnp.dot(rows_ref[...], uw[:, n : n + size], preferred_element_type=F32)
+            gate_act = dot_t(rows_ref[...], gw[n : n + size, :])
+            up_act = dot_t(rows_ref[...], uw[n : n + size, :])
             hid[:, n : n + size] = silu_mul(gate_act, up_act)
 
     def rs_refs(b):
@@ -397,48 +403,48 @@
         total[...] += mix(combine(ring(b)), ret[b - 1])
 
     first, second, third = order
-    ag1(first)
     loads[0].wait()
     loads[1].wait()
     hidden(xloc)
-    ag1(second)
+    ag1(first)
     loads[2].wait()
     loads[3].wait()
     acts = jnp.dot(normed[...], dgu[...], preferred_element_type=F32)
     dhid[...] = silu_mul(acts[:, :dsp], acts[:, dsp:])
-    ag1(third)
-    ag2(first)
+    ag1(second)
     loads[4].wait()
     loads[5].wait()
     for copy in gcopies:
         copy.wait_recv()
     dense_partials()
+    ag2(first)
+    ag1(third)
     ag2(second)
     ag3(first)
     rs1(0)
+    ag2(third)
+    ag3(second)
     ag_done(first)
     hidden(xbuf.at[first - 1])
-    ag2(third)
-    ag3(second)
     partials(first)
+    ag3(third)
     rs2(0)
-    ag3(third)
     rs1(first)
     ag_done(second)
     hidden(xbuf.at[second - 1])
-    rs3(0)
     partials(second)
     rs2(first)
     rs1(second)
     ag_done(third)
     hidden(xbuf.at[third - 1])
+    partials(third)
     rs3(first)
-    partials(third)
     rs2(second)
     rs1(third)
+    rs3(0)
     rs3(second)
+    rs2(third)
     returned(first)
-    rs2(third)
     returned(second)
     rs3(third)
     returned(third)
@@ -477,13 +483,14 @@
         in_specs=[vmem] * 4 + [hbm] * 6 + [vmem],
         out_specs=vmem,
         scratch_shapes=[
-            pltpu.VMEM((width, ffp), BF),
-            pltpu.VMEM((width, ffp), BF),
+            pltpu.VMEM((ffp, width), BF),
+            pltpu.VMEM((ffp, width), BF),
             pltpu.VMEM((ffp, width), BF),
             pltpu.VMEM((width, 2 * dsp), BF),
             pltpu.VMEM((dsp, width), BF),
             pltpu.VMEM((group, width), BF),
             pltpu.VMEM((128, group), F32),
+            pltpu.VMEM((group, 128), F32),
             pltpu.VMEM((group, 128), F32),
             pltpu.VMEM((parts, 1, cols), F32),
             pltpu.VMEM((rounds, cap, cols), BF),
@@ -520,10 +527,10 @@
     )(
         tokens,
         norm_gain[None, :],
-        expert_ids,
-        routing_weight,
-        expert_gate,
-        expert_up,
+        expert_ids.T,
+        routing_weight.T,
+        jnp.swapaxes(expert_gate, 1, 2),
+        jnp.swapaxes(expert_up, 1, 2),
         expert_down,
         dense_gate_w,
         dense_up_w,

time: 70 us -> 57.9 us (0.83)
  local copies, waits for them, and re-layouts: 12.1 us -> 1.57 us
  Pallas kernels: 57.6 us -> 56.2 us
    unnamed x7 -> x1, local copies, waits for them, and re-layouts: 12.1 us -> 1.57 us
    pallas_call x1, Pallas kernels: 57.6 us -> 56.2 us  [fused_local(): pl.pallas_call(functools.partial(fused_kernel, experts), out_shape=jax.Sh...]
where the time goes in v2:
time: 57.9 us; the launch traced here: 57.8 us
  Pallas kernels  56.2 us (97%)
  local copies, waits for them, and re-layouts  1.57 us (3%)
    pallas_call x1, Pallas kernels, fused_local(): pl.pallas_call(functools.partial(fused_kernel, experts), out_shape=jax.Sh...  56.2 us
    unnamed x1, local copies, waits for them, and re-layouts  1.57 us

profile of v2, /device:TPU:0, one launch (start us, length us, event | category | flops | bytes accessed | tf_op | source)
XLA Modules:
  0.0 57.8 jit_solution(17117509056812122097)
XLA Ops:
  0.0 56.2 %routed_layer.1 = bf16[256,256]{1,0:T(8,128)(2,1)} custom-call(bf16[256,2048]{1,0:T(8,128)(2,1)} %tok_ref.1, f32[1,2048]{1,0:T(1,128)} %bitcast.8, s32[2,256]{1,0:T(2,128)} %bitcast.9, f32[2,256]{1,0:T(2,128)} %bitcast.10, bf16[1,704,2048]{2,1,0:T(8,128)(2,1)} %bitcast.6, bf16[1,704,2048]{2,1,0:T(8,128)(2,1)} %bitcast.7, bf16[1,704,2048]{2,1,0:T(8,128)(2,1)} %dw_hbm.1, ...), custom_call_target="tpu_custom_call" | custom-call | tf_op jit(solution)/shard_map/routed_layer/pallas_call | solution.py:480
  56.2 1.6 %copy.13 = bf16[256,256]{1,0:T(8,128)(2,1)} copy(bf16[256,256]{1,0:T(8,128)(2,1)} %routed_layer.1) | data formatting | bytes 262144
